TPU v7x, 32 devices: a whole 2x2x4 slice. The times are simulated.
32 devices in a mesh: ep: 8 (over z, x), tp: 4 (over y, core).
Axes of the slice: x: 2, y: 2, z: 4, core: 2. Of those that a mesh axis runs over, the one named last changes fastest.
Arguments:
- tokens: bfloat16 [32, 2048], P('ep'), may hold values from -6 to 6
- norm_gain: bfloat16 [2048], replicated, may hold values from 0.099609375 to 1.8984375
- in_weight: bfloat16 [2048, 1024], P(None, 'tp'), may hold values from -0.125 to 0.125
- decay_rate: float32 [64, 64], P('tp'), may hold values from 0.05 to 1
- frequency: float32 [64, 64], P('tp'), may hold values from -3 to 3
- log_step: float32 [64], P('tp'), may hold values from -2.3 to 0.7
- input_real: float32 [64, 64, 16], P('tp'), may hold values from -1.75 to 1.75
- input_imag: float32 [64, 64, 16], P('tp'), may hold values from -1.75 to 1.75
- output_real: float32 [64, 16, 64], P('tp'), may hold values from -0.5 to 0.5
- output_imag: float32 [64, 16, 64], P('tp'), may hold values from -0.5 to 0.5
- skip_gain: float32 [1024], P('tp'), may hold values from -3 to 3
- state_real: float32 [32, 64, 64], P('ep', 'tp'), may hold values from -6 to 6
- state_imag: float32 [32, 64, 64], P('ep', 'tp'), may hold values from -6 to 6
- out_weight: bfloat16 [1024, 2048], P('tp'), may hold values from -0.1875 to 0.1875
- ffn_gain: bfloat16 [2048], replicated, may hold values from 0.099609375 to 1.8984375
- expert_ids: int32 [32, 2], replicated, may hold values from 0 to 7, all different within a row; in each aligned block of 4 rows (0 to 3, 4 to 7, ...) at most 2 rows name the same one
- route_weights: float32 [32, 2], P('ep'), may hold values from 0.2 to 1
- gate_weight: bfloat16 [2048, 65536], P(None, ('ep', 'tp')), may hold values from -0.125 to 0.125
- up_weight: bfloat16 [2048, 65536], P(None, ('ep', 'tp')), may hold values from -0.125 to 0.125
- down_weight: bfloat16 [65536, 2048], P('ep', 'tp'), may hold values from -0.0625 to 0.0625
Outputs:
- mixed: bfloat16 [32, 2048], P('ep', 'tp')
- new_real: float32 [32, 64, 64], P('ep', 'tp')
- new_imag: float32 [32, 64, 64], P('ep', 'tp')
Inputs may be any that keep to these rules, and one draw needn't show every extreme that they name: `expert_ids`: the 2 experts of a row differ. In each aligned block of 4 rows (the rows of one index of ep) no expert is named by more than 2 rows, and in some blocks one expert is named by exactly 2 rows.
All inputs are finite; a program needn't handle non-finite values.
Results may differ from a plain program's by a relative error of at most 0.007.
Values may be sent and summed in bfloat16 or wider, within the bound.
A program may use at most 64 MiB of HBM per device.

v0:
```python
import jax
import jax.numpy as jnp
from jax import lax
from jax.sharding import PartitionSpec as P

EXPERTS = 8
EPSILON = 1e-06


def rms_scale(values, gain):
    floats = values.astype(jnp.float32)
    return (
        floats
        * lax.rsqrt(jnp.mean(floats * floats, axis=-1, keepdims=True) + EPSILON)
        * gain.astype(jnp.float32)
    )


def discretize(decay_rate, frequency, log_step, input_real, input_imag):
    step_size = jnp.exp(log_step)[:, None]
    lam_real = -decay_rate
    magnitude = jnp.exp(lam_real * step_size)
    turned = frequency * step_size
    bar_real = magnitude * jnp.cos(turned)
    bar_imag = magnitude * jnp.sin(turned)
    denom = lam_real * lam_real + frequency * frequency
    minus_one = bar_real - 1.0
    factor_real = (minus_one * lam_real + bar_imag * frequency) / denom
    factor_imag = (bar_imag * lam_real - minus_one * frequency) / denom
    b_real = factor_real[..., None] * input_real - factor_imag[..., None] * input_imag
    b_imag = factor_real[..., None] * input_imag + factor_imag[..., None] * input_real
    return (bar_real, bar_imag, b_real, b_imag)


def state_update(
    projected,
    state_real,
    state_imag,
    decay_rate,
    frequency,
    log_step,
    input_real,
    input_imag,
    output_real,
    output_imag,
    skip_gain,
):
    bar_real, bar_imag, b_real, b_imag = discretize(
        decay_rate, frequency, log_step, input_real, input_imag
    )
    count, groups, _ = state_real.shape
    high = lax.Precision.HIGHEST
    grouped = projected.astype(jnp.float32).reshape(count, groups, -1)
    drive_real = jnp.einsum("sgp,gnp->sgn", grouped, b_real, precision=high)
    drive_imag = jnp.einsum("sgp,gnp->sgn", grouped, b_imag, precision=high)
    new_real = bar_real * state_real - bar_imag * state_imag + drive_real
    new_imag = bar_real * state_imag + bar_imag * state_real + drive_imag
    readout = jnp.einsum("sgn,gpn->sgp", new_real, output_real, precision=high) - jnp.einsum(
        "sgn,gpn->sgp", new_imag, output_imag, precision=high
    )
    readout = readout.reshape(count, -1) + skip_gain * grouped.reshape(count, -1)
    return (jax.nn.gelu(readout).astype(jnp.bfloat16), new_real, new_imag)


def slot_table(own_ids, own_weights, slot_count):
    expert_range = jnp.arange(EXPERTS, dtype=jnp.int32)
    onehot = (own_ids[:, :, None] == expert_range).astype(jnp.int32)
    flat = onehot.reshape(-1, EXPERTS)
    before = (jnp.cumsum(flat, axis=0) - flat).reshape(onehot.shape)
    slots = jnp.arange(slot_count, dtype=jnp.int32)
    match = (before[..., None] == slots) & (onehot[..., None] > 0)
    table = jnp.sum(jnp.where(match, own_weights[:, :, None, None], 0.0), axis=1)
    return jnp.transpose(table, (1, 2, 0))


def shards(
    tokens,
    norm_gain,
    in_weight,
    decay_rate,
    frequency,
    log_step,
    input_real,
    input_imag,
    output_real,
    output_imag,
    skip_gain,
    state_real,
    state_imag,
    out_weight,
    ffn_gain,
    expert_ids,
    route_weights,
    gate_weight,
    up_weight,
    down_weight,
):
    normed_in = rms_scale(tokens, norm_gain).astype(jnp.bfloat16)
    projected = jnp.dot(normed_in, in_weight, preferred_element_type=jnp.float32).astype(
        jnp.bfloat16
    )
    activated, new_real, new_imag = state_update(
        projected,
        state_real,
        state_imag,
        decay_rate,
        frequency,
        log_step,
        input_real,
        input_imag,
        output_real,
        output_imag,
        skip_gain,
    )
    delta = lax.psum(jnp.dot(activated, out_weight, preferred_element_type=jnp.float32), "tp")
    hidden_state = (tokens.astype(jnp.float32) + delta).astype(jnp.bfloat16)
    normed = rms_scale(hidden_state, ffn_gain).astype(jnp.bfloat16)
    seq_count, width = normed.shape
    slot_count = seq_count // 2
    group_span = lax.axis_size("ep") // EXPERTS
    my_index = lax.axis_index("ep")
    own_ids = lax.dynamic_slice_in_dim(expert_ids, my_index * seq_count, seq_count, 0)
    unit_weights = jnp.ones(own_ids.shape, jnp.float32)
    select = slot_table(own_ids, unit_weights, slot_count)
    outgoing = jnp.einsum(
        "xcs,sd->xcd", select.astype(jnp.bfloat16), normed, preferred_element_type=jnp.float32
    ).astype(jnp.bfloat16)
    received = lax.all_to_all(
        jnp.repeat(outgoing, group_span, axis=0), "ep", split_axis=0, concat_axis=0, tiled=True
    )
    slot_rows = received.reshape(-1, width)
    gate_pre = jnp.dot(slot_rows, gate_weight, preferred_element_type=jnp.float32)
    up_pre = jnp.dot(slot_rows, up_weight, preferred_element_type=jnp.float32)
    hidden = (jax.nn.silu(gate_pre) * up_pre).astype(jnp.bfloat16)
    quarter = down_weight.shape[1]
    partial_out = jnp.dot(
        lax.all_gather(hidden, "tp", axis=1, tiled=True),
        down_weight,
        preferred_element_type=jnp.float32,
    )
    rounded = partial_out.astype(jnp.bfloat16).reshape(-1, slot_count, quarter)
    returned = lax.all_to_all(rounded, "ep", split_axis=0, concat_axis=0, tiled=True)
    summed = (
        returned.astype(jnp.float32).reshape(EXPERTS, group_span, slot_count, quarter).sum(axis=1)
    )
    weight_table = slot_table(own_ids, route_weights, slot_count)
    routed = jnp.einsum("xcs,xcd->sd", weight_table, summed, precision=lax.Precision.HIGHEST)
    residual = lax.dynamic_slice_in_dim(hidden_state, lax.axis_index("tp") * quarter, quarter, 1)
    mixed = (residual.astype(jnp.float32) + routed).astype(jnp.bfloat16)
    return (mixed, new_real, new_imag)


def solution(mesh):
    in_specs = (
        P("ep", None),
        P(),
        P(None, "tp"),
        P("tp", None),
        P("tp", None),
        P("tp"),
        P("tp", None, None),
        P("tp", None, None),
        P("tp", None, None),
        P("tp", None, None),
        P("tp"),
        P("ep", "tp", None),
        P("ep", "tp", None),
        P("tp", None),
        P(),
        P(),
        P("ep", None),
        P(None, ("ep", "tp")),
        P(None, ("ep", "tp")),
        P("ep", "tp"),
    )
    out_specs = (P("ep", "tp"), P("ep", "tp", None), P("ep", "tp", None))
    return jax.shard_map(shards, mesh=mesh, in_specs=in_specs, out_specs=out_specs, check_vma=False)
```

profile of v0, /device:TPU:0, one launch (start us, length us, event | category | flops | bytes accessed | tf_op | source)
XLA Modules:
  0.0 71.3 jit_solution(13652618909060821899)
XLA Ops:
  0.7 0.8 %constant_dynamic-slice_fusion = s32[4,2]{0,1:T(2,128)S(1)} fusion(s32[32,2]{0,1:T(2,128)} %param.35, s32[]{:T(128)S(6)} %select_n.14), kind=kLoop, calls=%fused_computation.78 | loop fusion | bytes 68 | tf_op jit(solution)/shard_map/dynamic_slice | solution.py:122
  1.5 0.1 copy.71
  1.6 0.1 eq.56
  1.7 0.7 exp.10
  2.4 0.9 %fusion.19 = f32[4]{0:T(128)S(1)} fusion(bf16[4,2048]{1,0:T(4,128)(2,1)} %param.20), kind=kLoop, calls=%fused_computation.32 | loop fusion | flops 24572 | bytes 16400 | tf_op jit(solution)/shard_map/reduce_sum | solution.py:14
  3.3 0.7 convert_element_type.68
  4.0 1.5 %convolution_convert_fusion.2 = bf16[4,256]{1,0:T(4,128)(2,1)S(1)} fusion(bf16[2048,256]{1,0:T(8,128)(2,1)} %param.22, bf16[4,2048]{1,0:T(4,128)(2,1)} %param.20, f32[2048]{0:T(1024)S(1)} %convert_element_type.68, f32[4]{0:T(128)S(1)} %add_rsqrt_fusion.1), kind=kOutput, calls=%fused_computation.13 | convolution fusion | flops 4228096 | bytes 1075216 | tf_op jit(solution)/shard_map/dot_general | solution.py:99
  5.5 0.1 reshape.72
  5.6 0.8 %cosine_multiply_fusion = (f32[16,64]{1,0:T(8,128)S(1)}, f32[16,64]{1,0:T(8,128)S(1)}, f32[16,64]{1,0:T(8,128)S(1)}, f32[16,64]{1,0:T(8,128)S(1)}) fusion(f32[16,64]{1,0:T(8,128)} %param.24, f32[16,64]{1,0:T(8,128)} %param.23, f32[16]{0:T(128)S(1)} %exp.10), kind=kLoop, calls=%fused_computation.51 | loop fusion | flops 17408 | bytes 24640 | tf_op jit(solution)/shard_map/mul | solution.py:24
  6.4 1.2 %fusion.2 = f32[4,16,64]{2,0,1:T(4,128)S(1)} fusion(f32[16,64,16]{1,2,0:T(8,128)} %param.26, f32[16,64,16]{1,2,0:T(8,128)} %param.27, f32[16,64]{1,0:T(8,128)S(1)} %get-tuple-element.21, f32[16,64]{1,0:T(8,128)S(1)} %get-tuple-element.20, f32[4,16,64]{2,1,0:T(8,128)} %param.32, f32[4,16,64]{2,1,0:T(8,128)} %param.31, f32[16,64]{1,0:T(8,128)S(1)} %get-tuple-element.22, ...), kind=kOutput, calls=%fused_computation.6 | convolution fusion | flops 851968 | bytes 198656 | tf_op jit(solution)/shard_map/sgp,gnp->sgn/dot_general | solution.py:55
  7.6 1.2 %fusion.3 = f32[4,16,64]{2,0,1:T(4,128)S(1)} fusion(f32[16,64,16]{1,2,0:T(8,128)} %param.27, f32[16,64,16]{1,2,0:T(8,128)} %param.26, f32[16,64]{1,0:T(8,128)S(1)} %get-tuple-element.21, f32[16,64]{1,0:T(8,128)S(1)} %get-tuple-element.20, f32[4,16,64]{2,1,0:T(8,128)} %param.32, f32[4,16,64]{2,1,0:T(8,128)} %param.31, f32[16,64]{1,0:T(8,128)S(1)} %get-tuple-element.22, ...), kind=kOutput, calls=%fused_computation.8 | convolution fusion | flops 851968 | bytes 198656 | tf_op jit(solution)/shard_map/sgp,gnp->sgn/dot_general | solution.py:54
  8.9 0.1 fusion.43
  9.0 0.7 convert_element_type.80
  9.7 1.2 %fusion.60 = f32[16,4,16]{2,1,0:T(4,128)S(1)} fusion(f32[4,16,64]{2,0,1:T(4,128)S(1)} %fusion.3, f32[16,16,64]{2,1,0:T(8,128)} %param.28), kind=kOutput, calls=%fused_computation.84 | convolution fusion | flops 786432 | bytes 86016 | tf_op jit(solution)/shard_map/sgn,gpn->sgp/dot_general | solution.py:58
  10.9 1.2 %fusion.1 = f32[4,16,16]{2,0,1:T(4,128)S(1)} fusion(f32[16,4,16]{2,1,0:T(4,128)S(1)} %fusion.60, f32[4,16,64]{2,0,1:T(4,128)S(1)} %fusion.2, f32[16,16,64]{2,1,0:T(8,128)} %param.29), kind=kOutput, calls=%fused_computation.4 | convolution fusion | flops 787456 | bytes 90112 | tf_op jit(solution)/shard_map/sgn,gpn->sgp/dot_general | solution.py:58
  12.1 0.1 reshape.73
  12.2 0.9 %fusion.46 = f32[4,2048]{1,0:T(4,128)S(1)} fusion(bf16[256,2048]{1,0:T(8,128)(2,1)S(1)} %copy-done, f32[4,256]{1,0:T(4,128)S(1)} %reshape.73, bf16[4,256]{1,0:T(4,128)(2,1)S(1)} %convolution_convert_fusion.2, f32[256]{0:T(256)} %param.30), kind=kOutput, calls=%fused_computation.69 | convolution fusion | flops 4206592 | bytes 1088512 | tf_op jit(solution)/shard_map/dot_general | solution.py:115
  13.2 12.9 %psum.7 = f32[4,2048]{1,0:T(4,128)S(1)} all-reduce(f32[4,2048]{1,0:T(4,128)S(1)} %fusion.46), channel_id=1, replica_groups=mesh['ep'=8,'tp'=4] {'tp'}, use_global_device_ids=true, to_apply=%region_1.0 | all-reduce | flops 8192 | bytes 65536 | tf_op jit(solution)/shard_map/psum | solution.py:115
  26.1 0.9 %fusion.16 = (f32[4]{0:T(128)S(1)}, bf16[4,2048]{1,0:T(4,128)(2,1)S(1)}) fusion(f32[4,2048]{1,0:T(4,128)S(1)} %psum.7, bf16[4,2048]{1,0:T(4,128)(2,1)} %param.20), kind=kLoop, calls=%fused_computation.29 | loop fusion | flops 49148 | bytes 65552 | tf_op jit(solution)/shard_map/reduce_sum | solution.py:14
  26.9 0.8 %select_reduce_fusion.1 = (f32[4,8,2]{1,0,2:T(4,128)S(1)}, bf16[4,8,2]{1,0,2:T(4,128)(2,1)S(1)}) fusion(f32[4,2]{0,1:T(2,128)} %param.36, s32[4,2,8]{2,0,1:T(4,128)S(1)} %copy.73, pred[4,2,8]{2,0,1:T(4,128)(4,1)S(1)} %copy.74), kind=kLoop, calls=%fused_computation.45 | loop fusion | flops 640 | bytes 736 | tf_op jit(solution)/shard_map/reduce_sum | solution.py:72
  27.7 0.2 convolution_convert_fusion
  28.0 12.5 %all_to_all.10 = bf16[8,2,2048]{2,1,0:T(2,128)(2,1)S(1)} all-to-all(bf16[8,2,2048]{2,1,0:T(2,128)(2,1)S(1)} %copy.75), channel_id=1, replica_groups=mesh['ep'=8,'tp'=4] {'ep'}, dimensions={0} | all-to-all | bytes 131072 | tf_op jit(solution)/shard_map/all_to_all | solution.py:128
  40.5 4.6 %fusion.61 = f32[16,2048]{1,0:T(8,128)S(1)} fusion(bf16[16,2048]{1,0:T(8,128)(2,1)S(1)} %reshape.74, bf16[2048,2048]{1,0:T(8,128)(2,1)} %param.37), kind=kOutput, calls=%fused_computation.85 | convolution fusion | flops 134217728 | bytes 8585216 | tf_op jit(solution)/shard_map/dot_general | solution.py:132
  45.1 4.6 %fusion = bf16[16,2048]{1,0:T(8,128)(2,1)S(1)} fusion(bf16[16,2048]{1,0:T(8,128)(2,1)S(1)} %reshape.74, bf16[2048,2048]{1,0:T(8,128)(2,1)} %param.38, f32[16,2048]{1,0:T(8,128)S(1)} %fusion.61), kind=kOutput, calls=%fused_computation.2 | convolution fusion | flops 134414336 | bytes 8650752 | tf_op jit(solution)/shard_map/dot_general | solution.py:133
  49.7 5.8 %all_gather.3 = bf16[16,8192]{1,0:T(8,128)(2,1)S(1)} all-gather(bf16[16,2048]{1,0:T(8,128)(2,1)S(1)} %fusion), channel_id=1, replica_groups=mesh['ep'=8,'tp'=4] {'tp'}, dimensions={1}, use_global_device_ids=true | all-gather | bytes 327680 | tf_op jit(solution)/shard_map/all_gather | solution.py:137
  55.5 4.6 %convolution_convert_fusion.1 = bf16[16,512]{1,0:T(8,128)(2,1)S(1)} fusion(bf16[16,8192]{1,0:T(8,128)(2,1)S(1)} %all_gather.3, bf16[8192,512]{1,0:T(8,128)(2,1)} %param.39), kind=kOutput, calls=%fused_computation.9 | convolution fusion | flops 134225920 | bytes 8667136 | tf_op jit(solution)/shard_map/dot_general | solution.py:136
  60.0 0.6 reshape.75
  60.7 3.3 %all-to-all-start.1 = ((bf16[8,2,512]{2,1,0:T(2,128)(2,1)}), bf16[8,2,512]{2,1,0:T(2,128)(2,1)S(1)}, u32[]{:S(2)}, u32[]{:S(2)}) async-start(bf16[8,2,512]{2,1,0:T(2,128)(2,1)} %reshape.75), calls=%async_computation.1 | async-start | bytes 32768 | tf_op jit(solution)/shard_map/all_to_all | solution.py:142
  64.0 0.6 copy.77
  64.6 0.6 copy.78
  65.2 5.3 %all-to-all-done.1 = bf16[8,2,512]{2,1,0:T(2,128)(2,1)S(1)} async-done(((bf16[8,2,512]{2,1,0:T(2,128)(2,1)}), bf16[8,2,512]{2,1,0:T(2,128)(2,1)S(1)}, u32[]{:S(2)}, u32[]{:S(2)}) %all-to-all-start.1) | async-done | bytes 16416 | tf_op jit(solution)/shard_map/all_to_all | solution.py:142
  70.5 0.8 %fusion.5 = bf16[4,512]{1,0:T(4,128)(2,1)} fusion(bf16[8,2,512]{2,1,0:T(2,128)(2,1)S(1)} %all-to-all-done.1, f32[4,8,2]{1,0,2:T(4,128)S(1)} %get-tuple-element.15, bf16[4,2048]{1,0:T(4,128)(2,1)S(1)} %get-tuple-element.18, s32[]{:T(128)S(6)} %select_n.13), kind=kOutput, calls=%fused_computation.12 | convolution fusion | flops 399360 | bytes 24836 | tf_op jit(solution)/shard_map/xcs,xcd->sd/dot_general | solution.py:147
  (12 shorter events, 0.3 us)
Async XLA Ops:
  0.6 11.6 %copy-start = (bf16[256,2048]{1,0:T(8,128)(2,1)S(1)}, bf16[256,2048]{1,0:T(8,128)(2,1)}, u32[]{:S(2)}) copy-start(bf16[256,2048]{1,0:T(8,128)(2,1)} %param.33) | copy-start | bytes 3145732
  60.7 9.9 %all-to-all-start.1 = ((bf16[8,2,512]{2,1,0:T(2,128)(2,1)}), bf16[8,2,512]{2,1,0:T(2,128)(2,1)S(1)}, u32[]{:S(2)}, u32[]{:S(2)}) async-start(bf16[8,2,512]{2,1,0:T(2,128)(2,1)} %reshape.75), calls=%async_computation.1 | async-start | bytes 32768 | tf_op jit(solution)/shard_map/all_to_all | solution.py:142
where the time goes:
time: 72.1 us; the launch traced here: 71.3 us
  blocking collectives  31.2 us (43%)
  matrix products  22 us (31%)
  waiting for transfers between devices  5.28 us (7%)
  other arithmetic  4.97 us (7%)
  local copies, waits for them, and re-layouts  3.84 us (5%)
  starting transfers between devices  3.33 us (5%)
  between operations  0.73 us (1%)
    psum x1, blocking collectives, shards(): lax.psum(jnp.dot(activated, out_weight, preferred_element_type=jnp.float3...  12.9 us
    all_to_all x1, blocking collectives, shards(): lax.all_to_all(jnp.repeat(outgoing, group_span, axis=0), 'ep', split_axis...  12.5 us
    all_gather x1, blocking collectives, shards(): lax.all_gather(hidden, 'tp', axis=1, tiled=True)  5.77 us
    all_to_all x1, waiting for transfers between devices, shards(): lax.all_to_all(rounded, 'ep', split_axis=0, concat_axis=0, tiled=True)  5.28 us
    dot_general x1, matrix products, shards(): up_pre = jnp.dot(slot_rows, up_weight, preferred_element_type=jnp.float32)  4.58 us
    dot_general x1, matrix products, shards(): jnp.dot(slot_rows, gate_weight, preferred_element_type=jnp.float32)  4.58 us
    dot_general x1, matrix products, shards(): jnp.dot(lax.all_gather(hidden, 'tp', axis=1, tiled=True), down_weight, pr...  4.56 us
    all_to_all x1, starting transfers between devices, shards(): lax.all_to_all(rounded, 'ep', split_axis=0, concat_axis=0, tiled=True)  3.33 us
  transfers between devices with their start and end apart: 1, of which 1 were waited for; matrix products, arithmetic and copies ran while one was open for 2% of the time, Pallas kernels for 0%

commit v1 on v0

--- a/solution.py
+++ b/solution.py
@@ -1,3 +1,4 @@
+import functools
 import jax
 import jax.numpy as jnp
 from jax import lax
@@ -5,6 +6,15 @@
 
 EXPERTS = 8
 EPSILON = 1e-06
+
+
+def handle_the_ratios(here_x, group_axis, dim_no):
+    later = tuple((here_x for _ in range(lax.axis_size(group_axis))))
+    work_now = lax.all_to_all(jnp.stack(later), group_axis, 0, 0)
+    return jnp.concatenate(work_now, axis=dim_no)
+
+
+handle_turns = functools.partial(handle_the_ratios, group_axis="tp", dim_no=1)
 
 
 def rms_scale(values, gain):
@@ -133,11 +143,7 @@
     up_pre = jnp.dot(slot_rows, up_weight, preferred_element_type=jnp.float32)
     hidden = (jax.nn.silu(gate_pre) * up_pre).astype(jnp.bfloat16)
     quarter = down_weight.shape[1]
-    partial_out = jnp.dot(
-        lax.all_gather(hidden, "tp", axis=1, tiled=True),
-        down_weight,
-        preferred_element_type=jnp.float32,
-    )
+    partial_out = jnp.dot(handle_turns(hidden), down_weight, preferred_element_type=jnp.float32)
     rounded = partial_out.astype(jnp.bfloat16).reshape(-1, slot_count, quarter)
     returned = lax.all_to_all(rounded, "ep", split_axis=0, concat_axis=0, tiled=True)
     summed = (

time: 72.1 us -> 69.4 us (0.963)
  matrix products: 22 us -> 15.4 us
  blocking collectives: 31.2 us -> 33.9 us
  local copies, waits for them, and re-layouts: 3.84 us -> 4.92 us
    all_to_all x0 -> x1, blocking collectives: none -> 8.52 us  [handle_the_ratios(): work_now = lax.all_to_all(jnp.stack(later), group_axis, 0, 0)]
    all_gather x1 -> x0, blocking collectives: 5.77 us -> none  [shards(): lax.all_gather(hidden, 'tp', axis=1, tiled=True)]
    dot_general x1, matrix products: 4.58 us -> 1.2 us  [shards(): up_pre = jnp.dot(slot_rows, up_weight, preferred_element_type=jnp.float32)]
    dot_general x1, matrix products: 4.56 us -> 1.18 us  [shards(): jnp.dot(handle_turns(hidden), down_weight, preferred_element_type=jnp.flo...]
    unnamed x4 -> x10, local copies, waits for them, and re-layouts: 1.24 us -> 2.28 us
where the time goes in v1:
time: 69.4 us; the launch traced here: 68.6 us
  blocking collectives  33.9 us (49%)
  matrix products  15.4 us (22%)
  waiting for transfers between devices  5.28 us (8%)
  other arithmetic  4.97 us (7%)
  local copies, waits for them, and re-layouts  4.92 us (7%)
  starting transfers between devices  3.33 us (5%)
  between operations  0.78 us (1%)
    psum x1, blocking collectives, shards(): lax.psum(jnp.dot(activated, out_weight, preferred_element_type=jnp.float3...  12.9 us
    all_to_all x1, blocking collectives, shards(): lax.all_to_all(jnp.repeat(outgoing, group_span, axis=0), 'ep', split_axis...  12.5 us
    all_to_all x1, blocking collectives, handle_the_ratios(): work_now = lax.all_to_all(jnp.stack(later), group_axis, 0, 0)  8.52 us
    all_to_all x1, waiting for transfers between devices, shards(): lax.all_to_all(rounded, 'ep', split_axis=0, concat_axis=0, tiled=True)  5.28 us
    dot_general x1, matrix products, shards(): jnp.dot(slot_rows, gate_weight, preferred_element_type=jnp.float32)  4.73 us
    all_to_all x1, starting transfers between devices, shards(): lax.all_to_all(rounded, 'ep', split_axis=0, concat_axis=0, tiled=True)  3.33 us
    unnamed x10, local copies, waits for them, and re-layouts  2.28 us
    reduce_sum x2, other arithmetic, rms_scale(): jnp.mean(floats * floats, axis=-1, keepdims=True) + EPSILON  1.7 us
  transfers between devices with their start and end apart: 1, of which 1 were waited for; matrix products, arithmetic and copies ran while one was open for 2% of the time, Pallas kernels for 0%

profile of v1, /device:TPU:0, one launch (start us, length us, event | category | flops | bytes accessed | tf_op | source)
XLA Modules:
  0.0 68.6 jit_solution(2072003594796778317)
XLA Ops:
  0.7 0.8 %constant_dynamic-slice_fusion = s32[4,2]{0,1:T(2,128)S(1)} fusion(s32[32,2]{0,1:T(2,128)} %param.35, s32[]{:T(128)S(6)} %select_n.14), kind=kLoop, calls=%fused_computation.78 | loop fusion | bytes 68 | tf_op jit(solution)/shard_map/dynamic_slice | solution.py:132
  1.5 0.1 copy.72
  1.6 0.1 eq.56
  1.7 0.7 exp.10
  2.4 0.9 %fusion.19 = f32[4]{0:T(128)S(1)} fusion(bf16[4,2048]{1,0:T(4,128)(2,1)} %param.20), kind=kLoop, calls=%fused_computation.32 | loop fusion | flops 24572 | bytes 16400 | tf_op jit(solution)/shard_map/reduce_sum | solution.py:24
  3.3 0.7 %convert_element_type.68 = f32[2048]{0:T(1024)S(1)} convert(bf16[2048]{0:T(1024)(128)(2,1)} %param.21) | non-fusion elementwise | flops 2048 | bytes 12288 | tf_op jit(solution)/shard_map/convert_element_type | solution.py:25
  4.0 1.5 %convolution_convert_fusion.2 = bf16[4,256]{1,0:T(4,128)(2,1)S(1)} fusion(bf16[2048,256]{1,0:T(8,128)(2,1)} %param.22, bf16[4,2048]{1,0:T(4,128)(2,1)} %param.20, f32[2048]{0:T(1024)S(1)} %convert_element_type.68, f32[4]{0:T(128)S(1)} %add_rsqrt_fusion.1), kind=kOutput, calls=%fused_computation.13 | convolution fusion | flops 4228096 | bytes 1075216 | tf_op jit(solution)/shard_map/dot_general | solution.py:109
  5.5 0.1 reshape.80
  5.6 0.8 %cosine_multiply_fusion = (f32[16,64]{1,0:T(8,128)S(1)}, f32[16,64]{1,0:T(8,128)S(1)}, f32[16,64]{1,0:T(8,128)S(1)}, f32[16,64]{1,0:T(8,128)S(1)}) fusion(f32[16,64]{1,0:T(8,128)} %param.24, f32[16,64]{1,0:T(8,128)} %param.23, f32[16]{0:T(128)S(1)} %exp.10), kind=kLoop, calls=%fused_computation.51 | loop fusion | flops 17408 | bytes 24640 | tf_op jit(solution)/shard_map/mul | solution.py:34
  6.4 1.2 %fusion.2 = f32[4,16,64]{2,0,1:T(4,128)S(1)} fusion(f32[16,64,16]{1,2,0:T(8,128)} %param.26, f32[16,64,16]{1,2,0:T(8,128)} %param.27, f32[16,64]{1,0:T(8,128)S(1)} %get-tuple-element.21, f32[16,64]{1,0:T(8,128)S(1)} %get-tuple-element.20, f32[4,16,64]{2,1,0:T(8,128)} %param.32, f32[4,16,64]{2,1,0:T(8,128)} %param.31, f32[16,64]{1,0:T(8,128)S(1)} %get-tuple-element.22, ...), kind=kOutput, calls=%fused_computation.6 | convolution fusion | flops 851968 | bytes 198656 | tf_op jit(solution)/shard_map/sgp,gnp->sgn/dot_general | solution.py:65
  7.6 1.2 %fusion.3 = f32[4,16,64]{2,0,1:T(4,128)S(1)} fusion(f32[16,64,16]{1,2,0:T(8,128)} %param.27, f32[16,64,16]{1,2,0:T(8,128)} %param.26, f32[16,64]{1,0:T(8,128)S(1)} %get-tuple-element.21, f32[16,64]{1,0:T(8,128)S(1)} %get-tuple-element.20, f32[4,16,64]{2,1,0:T(8,128)} %param.32, f32[4,16,64]{2,1,0:T(8,128)} %param.31, f32[16,64]{1,0:T(8,128)S(1)} %get-tuple-element.22, ...), kind=kOutput, calls=%fused_computation.8 | convolution fusion | flops 851968 | bytes 198656 | tf_op jit(solution)/shard_map/sgp,gnp->sgn/dot_general | solution.py:64
  9.0 0.7 %convert_element_type.80 = f32[2048]{0:T(1024)S(1)} convert(bf16[2048]{0:T(1024)(128)(2,1)} %param.34) | non-fusion elementwise | flops 2048 | bytes 12288 | tf_op jit(solution)/shard_map/convert_element_type | solution.py:25
  9.7 1.2 %fusion.60 = f32[16,4,16]{2,1,0:T(4,128)S(1)} fusion(f32[4,16,64]{2,0,1:T(4,128)S(1)} %fusion.3, f32[16,16,64]{2,1,0:T(8,128)} %param.28), kind=kOutput, calls=%fused_computation.84 | convolution fusion | flops 786432 | bytes 86016 | tf_op jit(solution)/shard_map/sgn,gpn->sgp/dot_general | solution.py:68
  10.9 1.2 %fusion.1 = f32[4,16,16]{2,0,1:T(4,128)S(1)} fusion(f32[16,4,16]{2,1,0:T(4,128)S(1)} %fusion.60, f32[4,16,64]{2,0,1:T(4,128)S(1)} %fusion.2, f32[16,16,64]{2,1,0:T(8,128)} %param.29), kind=kOutput, calls=%fused_computation.4 | convolution fusion | flops 787456 | bytes 90112 | tf_op jit(solution)/shard_map/sgn,gpn->sgp/dot_general | solution.py:68
  12.1 0.1 reshape.81
  12.2 0.9 %fusion.46 = f32[4,2048]{1,0:T(4,128)S(1)} fusion(bf16[256,2048]{1,0:T(8,128)(2,1)S(1)} %copy-done, f32[4,256]{1,0:T(4,128)S(1)} %reshape.81, bf16[4,256]{1,0:T(4,128)(2,1)S(1)} %convolution_convert_fusion.2, f32[256]{0:T(256)} %param.30), kind=kOutput, calls=%fused_computation.69 | convolution fusion | flops 4206592 | bytes 1088512 | tf_op jit(solution)/shard_map/dot_general | solution.py:125
  13.2 12.9 %psum.7 = f32[4,2048]{1,0:T(4,128)S(1)} all-reduce(f32[4,2048]{1,0:T(4,128)S(1)} %fusion.46), channel_id=1, replica_groups=mesh['ep'=8,'tp'=4] {'tp'}, use_global_device_ids=true, to_apply=%region_1.0 | all-reduce | flops 8192 | bytes 65536 | tf_op jit(solution)/shard_map/psum | solution.py:125
  26.1 0.9 %fusion.16 = (f32[4]{0:T(128)S(1)}, bf16[4,2048]{1,0:T(4,128)(2,1)S(1)}) fusion(f32[4,2048]{1,0:T(4,128)S(1)} %psum.7, bf16[4,2048]{1,0:T(4,128)(2,1)} %param.20), kind=kLoop, calls=%fused_computation.29 | loop fusion | flops 49148 | bytes 65552 | tf_op jit(solution)/shard_map/reduce_sum | solution.py:24
  26.9 0.8 %select_reduce_fusion.1 = (f32[4,8,2]{1,0,2:T(4,128)S(1)}, bf16[4,8,2]{1,0,2:T(4,128)(2,1)S(1)}) fusion(f32[4,2]{0,1:T(2,128)} %param.36, s32[4,2,8]{2,0,1:T(4,128)S(1)} %copy.74, pred[4,2,8]{2,0,1:T(4,128)(4,1)S(1)} %copy.75), kind=kLoop, calls=%fused_computation.45 | loop fusion | flops 640 | bytes 736 | tf_op jit(solution)/shard_map/reduce_sum | solution.py:82
  27.7 0.2 convolution_convert_fusion
  28.0 12.5 %all_to_all.15 = bf16[8,2,2048]{2,1,0:T(2,128)(2,1)S(1)} all-to-all(bf16[8,2,2048]{2,1,0:T(2,128)(2,1)S(1)} %copy.76), channel_id=1, replica_groups=mesh['ep'=8,'tp'=4] {'ep'}, dimensions={0} | all-to-all | bytes 131072 | tf_op jit(solution)/shard_map/all_to_all | solution.py:138
  40.6 4.7 %fusion.61 = f32[16,2048]{1,0:T(8,128)S(1)} fusion(bf16[16,2048]{1,0:T(8,128)(2,1)S(1)} %reshape.82, bf16[2048,2048]{1,0:T(8,128)(2,1)} %param.37), kind=kOutput, calls=%fused_computation.85 | convolution fusion | flops 134217728 | bytes 8585216 | tf_op jit(solution)/shard_map/dot_general | solution.py:142
  45.3 1.0 %copy-done.1 = bf16[2048,2048]{1,0:T(8,128)(2,1)S(1)} copy-done((bf16[2048,2048]{1,0:T(8,128)(2,1)S(1)}, bf16[2048,2048]{1,0:T(8,128)(2,1)}, u32[]{:S(2)}) %copy-start.1) | copy-done | bytes 8388632
  46.3 1.2 %fusion = bf16[16,2048]{1,0:T(8,128)(2,1)S(1)} fusion(bf16[16,2048]{1,0:T(8,128)(2,1)S(1)} %reshape.82, bf16[2048,2048]{1,0:T(8,128)(2,1)S(1)} %copy-done.1, f32[16,2048]{1,0:T(8,128)S(1)} %fusion.61), kind=kOutput, calls=%fused_computation.2 | convolution fusion | flops 134414336 | bytes 8650752 | tf_op jit(solution)/shard_map/dot_general | solution.py:143
  47.5 8.5 %all_to_all.16 = bf16[4,16,2048]{2,1,0:T(8,128)(2,1)S(1)} all-to-all(bf16[4,16,2048]{2,1,0:T(8,128)(2,1)S(1)} %stack.2), channel_id=1, replica_groups=mesh['ep'=8,'tp'=4] {'tp'}, dimensions={0} | all-to-all | bytes 524288 | tf_op jit(solution)/shard_map/all_to_all | solution.py:13
  56.1 1.2 %convolution_convert_fusion.1 = bf16[16,512]{1,0:T(8,128)(2,1)S(1)} fusion(bf16[16,8192]{1,0:T(8,128)(2,1)S(1)} %bitcast.43, bf16[8192,512]{1,0:T(8,128)(2,1)S(1)} %bitcast.42), kind=kOutput, calls=%fused_computation.9 | convolution fusion | flops 134225920 | bytes 8667136 | tf_op jit(solution)/shard_map/dot_general | solution.py:146
  57.3 0.6 reshape.85
  57.9 3.3 %all-to-all-start.2 = ((bf16[8,2,512]{2,1,0:T(2,128)(2,1)}), bf16[8,2,512]{2,1,0:T(2,128)(2,1)S(1)}, u32[]{:S(2)}, u32[]{:S(2)}) async-start(bf16[8,2,512]{2,1,0:T(2,128)(2,1)} %reshape.85), calls=%async_computation.2 | async-start | bytes 32768 | tf_op jit(solution)/shard_map/all_to_all | solution.py:148
  61.3 0.6 copy.79
  61.9 0.6 copy.80
  62.5 5.3 %all-to-all-done.2 = bf16[8,2,512]{2,1,0:T(2,128)(2,1)S(1)} async-done(((bf16[8,2,512]{2,1,0:T(2,128)(2,1)}), bf16[8,2,512]{2,1,0:T(2,128)(2,1)S(1)}, u32[]{:S(2)}, u32[]{:S(2)}) %all-to-all-start.2) | async-done | bytes 16416 | tf_op jit(solution)/shard_map/all_to_all | solution.py:148
  67.8 0.8 %fusion.5 = bf16[4,512]{1,0:T(4,128)(2,1)} fusion(bf16[8,2,512]{2,1,0:T(2,128)(2,1)S(1)} %all-to-all-done.2, f32[4,8,2]{1,0,2:T(4,128)S(1)} %get-tuple-element.15, bf16[4,2048]{1,0:T(4,128)(2,1)S(1)} %get-tuple-element.18, s32[]{:T(128)S(6)} %select_n.13), kind=kOutput, calls=%fused_computation.12 | convolution fusion | flops 399360 | bytes 24836 | tf_op jit(solution)/shard_map/xcs,xcd->sd/dot_general | solution.py:153
  (21 shorter events, 0.4 us)
Async XLA Ops:
  0.6 11.6 %copy-start = (bf16[256,2048]{1,0:T(8,128)(2,1)S(1)}, bf16[256,2048]{1,0:T(8,128)(2,1)}, u32[]{:S(2)}) copy-start(bf16[256,2048]{1,0:T(8,128)(2,1)} %param.33) | copy-start | bytes 3145732
  40.5 5.8 %copy-start.1 = (bf16[2048,2048]{1,0:T(8,128)(2,1)S(1)}, bf16[2048,2048]{1,0:T(8,128)(2,1)}, u32[]{:S(2)}) copy-start(bf16[2048,2048]{1,0:T(8,128)(2,1)} %param.38) | copy-start | bytes 25165828
  40.6 15.5 %slice-start = ((s8[8388608]{0:T(1024)(128)(4,1)}), s8[4194304]{0:T(1024)(128)(4,1)S(1)}, s32[]{:S(2)}) async-start(s8[8388608]{0:T(1024)(128)(4,1)} %bitcast.41), calls=%async_computation.3 | async-start | bytes 8388608
  46.3 9.8 %slice-start.1 = ((s8[8388608]{0:T(1024)(128)(4,1)}), s8[4194304]{0:T(1024)(128)(4,1)S(1)}, s32[]{:S(2)}) async-start(s8[8388608]{0:T(1024)(128)(4,1)} %bitcast.41), calls=%async_computation.4 | async-start | bytes 8388608
  57.9 9.9 %all-to-all-start.2 = ((bf16[8,2,512]{2,1,0:T(2,128)(2,1)}), bf16[8,2,512]{2,1,0:T(2,128)(2,1)S(1)}, u32[]{:S(2)}, u32[]{:S(2)}) async-start(bf16[8,2,512]{2,1,0:T(2,128)(2,1)} %reshape.85), calls=%async_computation.2 | async-start | bytes 32768 | tf_op jit(solution)/shard_map/all_to_all | solution.py:148
